TPU v7x, 32 devices: a whole 2x2x4 slice. The times are simulated.
32 devices in a mesh: grp: 2 (over y), sp: 4 (over z), tp: 4 (over x, core).
Axes of the slice: x: 2, y: 2, z: 4, core: 2. Of those that a mesh axis runs over, the one named last changes fastest.
Arguments:
- stream: bfloat16 [2048, 2048], P(('grp', 'sp'), 'tp'), parts along dimension 0, may hold values from -1.5 to 1.5
- layer_norm_gain: float32 [2, 2048], replicated, may hold values from 0.1 to 1.9
- convolution_in_weight: bfloat16 [2, 2048, 1536], P(None, 'sp', 'tp'), may hold values from -0.125 to 0.125
- gating_in_weight: bfloat16 [2, 2048, 1536], P(None, 'sp', 'tp'), may hold values from -0.125 to 0.125
- output_weight: bfloat16 [2, 1536, 2048], P(None, 'tp', 'sp'), may hold values from -0.15625 to 0.15625
- convolution_kernel_taps: float32 [2, 4, 1536], P(None, None, 'tp'), may hold values from -12 to 12
- recurrent_gate_blocks: bfloat16 [2, 2, 2, 12, 128, 128], P(None, None, None, 'tp'), may hold values from -0.5 to 0.5
- channel_decay_logit: float32 [2, 2, 1536], P(None, None, 'tp')
- position_decay_boost: float32 [2, 2, 2048], P(None, None, ('grp', 'sp')), parts along dimension 2, may hold values from -1.4 to 0, as said below
Outputs:
- new_stream: bfloat16 [2048, 2048], P(('grp', 'sp'), 'tp'), parts along dimension 0
There are 2 independent parts, one for each index of `grp`. A program takes and returns all parts, laid end to end along the dimension named above; an argument that names none is the same for every part. Nothing has to cross between parts.
Inputs may be any that keep to these rules, and one draw needn't show every extreme that they name: `position_decay_boost`: zero at all but a few positions.
All inputs are finite; a program needn't handle non-finite values.
Results may differ from a plain program's by a relative error of at most 0.025.
Values may be sent and summed in bfloat16 or wider, within the bound.
A program may use at most 128 MiB of HBM per device.

v0:
```python
import jax
import jax.numpy as jnp
from jax import lax
from jax.sharding import PartitionSpec as P

EPS = 1e-06
RECURRENT_WIDTH = 8.0


def extended(cells, sides, width):
    for axis, dim in sides:
        count = lax.axis_size(axis)
        ends = count - 1
        head = lax.slice_in_dim(cells, 0, width, axis=dim)
        tail = lax.slice_in_dim(cells, cells.shape[dim] - width, cells.shape[dim], axis=dim)
        cells = jnp.concatenate(
            [
                lax.ppermute(tail, axis, [(i, (i + 1) % count) for i in range(ends)]),
                cells,
                lax.ppermute(head, axis, [((i + 1) % count, i) for i in range(ends)]),
            ],
            axis=dim,
        )
    return cells


def carried_in(part, axis, combine, identity, reverse):
    count = lax.axis_size(axis)
    place = lax.axis_index(axis)
    ahead = count - 1 - place if reverse else place
    gathered = jax.tree.map(lambda a: lax.all_gather(a, axis), part)
    state = jax.tree.map(lambda a, e: jnp.zeros_like(a) + jnp.asarray(e, a.dtype), part, identity)

    def one(step, state):
        source = count - 1 - step if reverse else step
        return combine(
            state, jax.tree.map(lambda a: lax.dynamic_index_in_dim(a, source, 0, False), gathered)
        )

    return lax.fori_loop(0, ahead, one, state)


def rms_norm(values, gain_row):
    floats = values.astype(jnp.float32)
    inverse = lax.rsqrt(jnp.mean(floats * floats, axis=-1, keepdims=True) + EPS)
    return (floats * inverse * gain_row).astype(jnp.bfloat16)


def combine_pairs(earlier, latter):
    return (earlier[0] * latter[0], latter[0] * earlier[1] + latter[1])


def local(
    stream,
    layer_norm_gain,
    convolution_in_weight,
    gating_in_weight,
    output_weight,
    convolution_kernel_taps,
    recurrent_gate_blocks,
    channel_decay_logit,
    position_decay_boost,
):
    tok_rows = stream.shape[0]
    channels = convolution_in_weight.shape[2]
    gate_count = recurrent_gate_blocks.shape[3]
    block_width = recurrent_gate_blocks.shape[4]
    seq_devices = lax.axis_size("sp")
    my_index = lax.axis_index("sp")
    seq_length = tok_rows * seq_devices
    positions = my_index * tok_rows + lax.iota(jnp.int32, tok_rows)
    at_first = (positions == 0)[:, None]
    at_last = (positions == seq_length - 1)[:, None]
    for layer_index in range(convolution_in_weight.shape[0]):
        features = lax.all_gather(stream, "tp", axis=1, tiled=True)
        normed = rms_norm(features, layer_norm_gain[layer_index])
        acc_x = jnp.dot(
            normed,
            lax.all_gather(convolution_in_weight[layer_index], "sp", axis=0, tiled=True),
            preferred_element_type=jnp.float32,
        )
        acc_y = jnp.dot(
            normed,
            lax.all_gather(gating_in_weight[layer_index], "sp", axis=0, tiled=True),
            preferred_element_type=jnp.float32,
        )
        proj_x = acc_x.astype(jnp.bfloat16)
        proj_y = acc_y.astype(jnp.bfloat16)
        padded = extended(proj_x, (("sp", 0),), 2).astype(jnp.float32)
        taps_now = convolution_kernel_taps[layer_index]
        conv_mixed = (
            taps_now[0] * padded[1 : tok_rows + 1]
            + taps_now[1] * padded[2 : tok_rows + 2]
            + taps_now[2] * padded[3 : tok_rows + 3]
            + taps_now[3] * padded[4 : tok_rows + 4]
        )
        convolution_output = conv_mixed.astype(jnp.bfloat16)
        conv_float = convolution_output.astype(jnp.float32)
        grouped = convolution_output.reshape(tok_rows, gate_count, block_width)
        results = []
        for scan_direction in range(2):
            gate_matrix_pair = recurrent_gate_blocks[layer_index, scan_direction]
            recurrent_branch = jax.nn.sigmoid(
                jnp.einsum(
                    "tnc,ncd->tnd", grouped, gate_matrix_pair[0], preferred_element_type=jnp.float32
                ).reshape(tok_rows, channels)
            )
            input_gate = jax.nn.sigmoid(
                jnp.einsum(
                    "tnc,ncd->tnd", grouped, gate_matrix_pair[1], preferred_element_type=jnp.float32
                ).reshape(tok_rows, channels)
            )
            decay_logarithm = (
                -RECURRENT_WIDTH
                * jax.nn.softplus(-channel_decay_logit[layer_index, scan_direction])
                * recurrent_branch
                + position_decay_boost[layer_index, scan_direction][:, None]
            )
            is_start = at_first if scan_direction == 0 else at_last
            multiplier = jnp.where(is_start, 1.0, jnp.sqrt(-jnp.expm1(2.0 * decay_logarithm)))
            driven = multiplier * input_gate * conv_float
            results.append(
                lax.associative_scan(
                    combine_pairs,
                    (jnp.exp(decay_logarithm), driven),
                    reverse=scan_direction == 1,
                    axis=0,
                )
            )
        cum_fwd, local_fwd = results[0]
        cum_bwd, local_bwd = results[1]
        identity = (jnp.ones((1, channels), jnp.float32), jnp.zeros((1, channels), jnp.float32))
        enter_fwd = carried_in(
            (cum_fwd[-1:], local_fwd[-1:]), "sp", combine_pairs, identity, False
        )[1]
        enter_bwd = carried_in((cum_bwd[:1], local_bwd[:1]), "sp", combine_pairs, identity, True)[1]
        state_sum = local_fwd + cum_fwd * enter_fwd + local_bwd + cum_bwd * enter_bwd
        gated = (state_sum * jax.nn.gelu(proj_y.astype(jnp.float32))).astype(jnp.bfloat16)
        partials = jnp.dot(
            gated,
            lax.all_gather(output_weight[layer_index], "sp", axis=1, tiled=True),
            preferred_element_type=jnp.float32,
        ).astype(jnp.bfloat16)
        branch_sum = lax.psum_scatter(
            partials.astype(jnp.float32).astype(jnp.bfloat16), "tp", scatter_dimension=1, tiled=True
        ).astype(jnp.float32)
        stream = (stream.astype(jnp.float32) + branch_sum).astype(jnp.bfloat16)
    return stream


def solution(mesh):
    return jax.shard_map(
        local,
        mesh=mesh,
        in_specs=(
            P(("grp", "sp"), "tp"),
            P(),
            P(None, "sp", "tp"),
            P(None, "sp", "tp"),
            P(None, "tp", "sp"),
            P(None, None, "tp"),
            P(None, None, None, "tp", None, None),
            P(None, None, "tp"),
            P(None, None, ("grp", "sp")),
        ),
        out_specs=P(("grp", "sp"), "tp"),
        check_vma=False,
    )
```

profile of v0, /device:TPU:0, one launch (start us, length us, event | category | flops | bytes accessed | tf_op | source)
XLA Modules:
  0.0 358.1 jit_solution(14976978191996592059)
XLA Ops:
  6.5 0.7 all-gather.31.cloned.1.call-update
  7.3 2.1 fusion.206
  9.5 1.0 fusion.207
  10.7 0.9 fusion.208
  15.3 13.0 %all-gather.31.cloned.1.call-done = bf16[256,2048]{1,0:T(8,128)(2,1)} async-done(((bf16[256,512]{1,0:T(8,128)(2,1)}), bf16[256,2048]{1,0:T(8,128)(2,1)}) %all-gather.31.cloned.1.call-update) | async-done | bytes 1048592 | tf_op jit(solution)/shard_map/all_gather | solution.py:75
  28.3 1.5 fusion
  29.9 37.1 %all-gather.35.cloned.1.call-done = bf16[1,2048,384]{2,1,0:T(8,128)(2,1)} async-done(((bf16[1,512,384]{2,1,0:T(8,128)(2,1)}), bf16[1,2048,384]{2,1,0:T(8,128)(2,1)}) %all-gather.35.cloned.1.call-update) | async-done | bytes 1572880 | tf_op jit(solution)/shard_map/all_gather | solution.py:79
  67.0 2.5 fusion.40
  69.5 2.6 collective-permute-start
  72.1 1.3 collective-permute-start.1
  73.5 4.2 %collective-permute-done.1 = bf16[2,384]{1,0:T(2,128)(2,1)S(1)} collective-permute-done((bf16[2,384]{1,0:T(2,128)(2,1)S(1)}, bf16[2,384]{1,0:T(2,128)(2,1)S(1)}, u32[]{:S(2)}, u32[]{:S(2)}) %collective-permute-start.1) | collective-permute-done | bytes 1568 | tf_op jit(solution)/shard_map/ppermute | solution.py:20
  80.0 1.6 convert_multiply_fusion.7
  87.3 12.3 %all-gather.15 = f32[4,1,384]{2,1,0:T(1,128)S(1)} all-gather(f32[1,1,384]{2,1,0:T(1,128)S(1)} %add_bitcast_fusion.6), channel_id=4, replica_groups=mesh['grp'=2,'sp'=4,'tp'=4] {'sp'}, dimensions={0}, use_global_device_ids=true | all-gather | bytes 7680 | tf_op jit(solution)/shard_map/all_gather | solution.py:31
  99.7 11.9 %all-gather.14 = f32[4,1,384]{2,1,0:T(1,128)S(1)} all-gather(f32[1,1,384]{2,1,0:T(1,128)S(1)} %add_bitcast_fusion.7), channel_id=3, replica_groups=mesh['grp'=2,'sp'=4,'tp'=4] {'sp'}, dimensions={0}, use_global_device_ids=true | all-gather | bytes 7680 | tf_op jit(solution)/shard_map/all_gather | solution.py:31
  116.5 1.6 pad.454
  118.1 0.8 add.988
  118.9 1.9 add.997
  120.8 0.7 add_bitcast_fusion.4
  121.5 12.5 %all-gather.17 = f32[4,1,384]{2,1,0:T(1,128)S(1)} all-gather(f32[1,1,384]{2,1,0:T(1,128)S(1)} %add_bitcast_fusion.4), channel_id=6, replica_groups=mesh['grp'=2,'sp'=4,'tp'=4] {'sp'}, dimensions={0}, use_global_device_ids=true | all-gather | bytes 7680 | tf_op jit(solution)/shard_map/all_gather | solution.py:31
  134.0 0.7 add_bitcast_fusion.5
  134.7 12.1 %all-gather.16 = f32[4,1,384]{2,1,0:T(1,128)S(1)} all-gather(f32[1,1,384]{2,1,0:T(1,128)S(1)} %add_bitcast_fusion.5), channel_id=5, replica_groups=mesh['grp'=2,'sp'=4,'tp'=4] {'sp'}, dimensions={0}, use_global_device_ids=true | all-gather | bytes 7680 | tf_op jit(solution)/shard_map/all_gather | solution.py:31
  146.9 2.6 rev.16
  149.5 2.6 rev.17
  152.2 4.4 %convolution_convert_fusion.1 = bf16[256,2048]{1,0:T(8,128)(2,1)} fusion(bf16[1,384,2048]{2,1,0:T(8,128)(2,1)} %all-gather.39.cloned.1.call-done, bf16[1,2048,384]{2,1,0:T(8,128)(2,1)} %all-gather.37.cloned.1.call-done, f32[256,384]{1,0:T(8,128)S(1)} %rev.17, f32[256,384]{1,0:T(8,128)S(1)} %rev.16, f32[256,384]{1,0:T(8,128)S(1)} %pad.422, ...), kind=kOutput, calls=%fused_computation.13 | convolution fusion | flops 809795584 | bytes 7614464 | tf_op jit(solution)/shard_map/dot_general | solution.py:139
  156.9 22.8 %reduce-scatter.3.cloned.1.call-done = bf16[256,512]{1,0:T(8,128)(2,1)} async-done(((bf16[256,2048]{1,0:T(8,128)(2,1)}), bf16[256,512]{1,0:T(8,128)(2,1)}) %reduce-scatter.3.cloned.1.call-update) | async-done | bytes 262160 | tf_op jit(solution)/shard_map/reduce_scatter | solution.py:144
  179.6 1.8 add_convert_fusion.1
  184.4 13.9 %all-gather.33.cloned.1.call-done = bf16[256,2048]{1,0:T(8,128)(2,1)} async-done(((bf16[256,512]{1,0:T(8,128)(2,1)}), bf16[256,2048]{1,0:T(8,128)(2,1)}) %all-gather.33.cloned.1.call-update) | async-done | bytes 1048592 | tf_op jit(solution)/shard_map/all_gather | solution.py:75
  198.3 1.5 fusion.3
  199.8 37.1 %all-gather.41.cloned.1.call-done = bf16[1,2048,384]{2,1,0:T(8,128)(2,1)} async-done(((bf16[1,512,384]{2,1,0:T(8,128)(2,1)}), bf16[1,2048,384]{2,1,0:T(8,128)(2,1)}) %all-gather.41.cloned.1.call-update) | async-done | bytes 1572880 | tf_op jit(solution)/shard_map/all_gather | solution.py:79
  236.9 2.5 fusion.49
  239.5 2.6 collective-permute-start.2
  242.1 1.3 collective-permute-start.3
  243.4 4.2 %collective-permute-done.3 = bf16[2,384]{1,0:T(2,128)(2,1)S(1)} collective-permute-done((bf16[2,384]{1,0:T(2,128)(2,1)S(1)}, bf16[2,384]{1,0:T(2,128)(2,1)S(1)}, u32[]{:S(2)}, u32[]{:S(2)}) %collective-permute-start.3) | collective-permute-done | bytes 1568 | tf_op jit(solution)/shard_map/ppermute | solution.py:20
  250.0 1.6 convert_multiply_fusion.5
  257.2 12.3 %all-gather.19 = f32[4,1,384]{2,1,0:T(1,128)S(1)} all-gather(f32[1,1,384]{2,1,0:T(1,128)S(1)} %add_bitcast_fusion.2), channel_id=11, replica_groups=mesh['grp'=2,'sp'=4,'tp'=4] {'sp'}, dimensions={0}, use_global_device_ids=true | all-gather | bytes 7680 | tf_op jit(solution)/shard_map/all_gather | solution.py:31
  269.7 11.9 %all-gather.18 = f32[4,1,384]{2,1,0:T(1,128)S(1)} all-gather(f32[1,1,384]{2,1,0:T(1,128)S(1)} %add_bitcast_fusion.3), channel_id=10, replica_groups=mesh['grp'=2,'sp'=4,'tp'=4] {'sp'}, dimensions={0}, use_global_device_ids=true | all-gather | bytes 7680 | tf_op jit(solution)/shard_map/all_gather | solution.py:31
  284.9 1.6 pad.518
  286.5 0.8 add.1076
  287.4 1.9 add.1085
  289.2 0.7 add_bitcast_fusion
  289.9 12.4 %all-gather.21 = f32[4,1,384]{2,1,0:T(1,128)S(1)} all-gather(f32[1,1,384]{2,1,0:T(1,128)S(1)} %add_bitcast_fusion), channel_id=13, replica_groups=mesh['grp'=2,'sp'=4,'tp'=4] {'sp'}, dimensions={0}, use_global_device_ids=true | all-gather | bytes 7680 | tf_op jit(solution)/shard_map/all_gather | solution.py:31
  302.3 0.7 add_bitcast_fusion.1
  303.0 12.1 %all-gather.20 = f32[4,1,384]{2,1,0:T(1,128)S(1)} all-gather(f32[1,1,384]{2,1,0:T(1,128)S(1)} %add_bitcast_fusion.1), channel_id=12, replica_groups=mesh['grp'=2,'sp'=4,'tp'=4] {'sp'}, dimensions={0}, use_global_device_ids=true | all-gather | bytes 7680 | tf_op jit(solution)/shard_map/all_gather | solution.py:31
  315.2 2.6 rev.18
  317.8 3.9 %rev.19 = f32[256,384]{1,0:T(8,128)} reverse(f32[256,384]{1,0:T(8,128)} %add.1085), dimensions={0} | reverse | bytes 786432 | tf_op jit(solution)/shard_map/rev | solution.py:123
  321.7 4.6 %convolution_convert_fusion = bf16[256,2048]{1,0:T(8,128)(2,1)} fusion(bf16[1,384,2048]{2,1,0:T(8,128)(2,1)} %all-gather.45.cloned.1.call-done, bf16[1,2048,384]{2,1,0:T(8,128)(2,1)} %all-gather.43.cloned.1.call-done, f32[256,384]{1,0:T(8,128)} %rev.19, f32[256,384]{1,0:T(8,128)S(1)} %rev.18, f32[256,384]{1,0:T(8,128)S(1)} %pad.486, ...), kind=kOutput, calls=%fused_computation.12 | convolution fusion | flops 809795584 | bytes 7614464 | tf_op jit(solution)/shard_map/dot_general | solution.py:139
  326.3 23.2 %reduce-scatter.5.cloned.1.call-done = bf16[256,512]{1,0:T(8,128)(2,1)} async-done(((bf16[256,2048]{1,0:T(8,128)(2,1)}), bf16[256,512]{1,0:T(8,128)(2,1)}) %reduce-scatter.5.cloned.1.call-update) | async-done | bytes 262160 | tf_op jit(solution)/shard_map/reduce_scatter | solution.py:144
  349.5 1.7 add_convert_fusion
  (646 shorter events, 29.0 us)
Async XLA Ops:
  6.5 2.9 copy-start.5
  6.5 21.8 %all-gather.31.cloned.1.call-start = ((), (), s32[]{:S(2)}) async-start(), calls=%async_computation.2 | async-start | bytes 1310720 | tf_op jit(solution)/shard_map/all_gather | solution.py:75
  7.3 59.7 %all-gather.35.cloned.1.call-start = ((), (), s32[]{:S(2)}) async-start(), calls=%async_computation.6 | async-start | bytes 1966080 | tf_op jit(solution)/shard_map/all_gather | solution.py:79
  9.4 1.3 copy-start.6
  9.4 142.7 %all-gather.37.cloned.1.call-start = ((), (), s32[]{:S(2)}) async-start(), calls=%async_computation.7 | async-start | bytes 1966080 | tf_op jit(solution)/shard_map/all_gather | solution.py:84
  10.4 1.2 copy-start.18
  10.4 1.8 copy-start.19
  10.4 2.5 copy-start.24
  10.4 3.7 %copy-start.29 = (f32[2,2,256]{2,1,0:T(2,128)S(1)}, f32[2,2,256]{2,1,0:T(2,128)}, u32[]{:S(2)}) copy-start(f32[2,2,256]{2,1,0:T(2,128)} %param.25) | copy-start | bytes 12292
  10.5 141.7 %all-gather.39.cloned.1.call-start = ((), (), s32[]{:S(2)}) async-start(), calls=%async_computation.8 | async-start | bytes 1966080 | tf_op jit(solution)/shard_map/all_gather | solution.py:141
  11.6 168.0 %reduce-scatter.3.cloned.1.call-start = ((), (), s32[]{:S(2)}) async-start(), calls=%async_computation.3 | async-start | bytes 1310720 | tf_op jit(solution)/shard_map/reduce_scatter | solution.py:144
  12.3 57.2 %copy-start.9 = (f32[1,2048]{1,0:T(1,128)}, f32[1,2048]{1,0:T(1,128)S(1)}, u32[]{:S(2)}) copy-start(f32[1,2048]{1,0:T(1,128)S(1)} %get-tuple-element.404) | copy-start | bytes 24580
  12.9 64.7 %copy-start.14 = (f32[384]{0:T(512)}, f32[384]{0:T(512)S(1)}, u32[]{:S(2)}) copy-start(f32[384]{0:T(512)S(1)} %get-tuple-element.267) | copy-start | bytes 4612
  12.9 64.7 %copy-start.15 = (f32[384]{0:T(512)}, f32[384]{0:T(512)S(1)}, u32[]{:S(2)}) copy-start(f32[384]{0:T(512)S(1)} %get-tuple-element.268) | copy-start | bytes 4612
  12.9 64.7 %copy-start.16 = (f32[384]{0:T(512)}, f32[384]{0:T(512)S(1)}, u32[]{:S(2)}) copy-start(f32[384]{0:T(512)S(1)} %get-tuple-element.269) | copy-start | bytes 4612
  12.9 64.8 %copy-start.17 = (f32[384]{0:T(512)}, f32[384]{0:T(512)S(1)}, u32[]{:S(2)}) copy-start(f32[384]{0:T(512)S(1)} %get-tuple-element.270) | copy-start | bytes 4612
  29.9 39.6 %copy-start.27 = (f32[256]{0:T(256)}, f32[256]{0:T(256)S(1)}, u32[]{:S(2)}) copy-start(f32[256]{0:T(256)S(1)} %add_rsqrt_fusion.1) | copy-start | bytes 3076
  69.5 8.6 %copy-start.30 = (bf16[2,2,2,3,128,128]{5,4,3,2,1,0:T(8,128)(2,1)S(1)}, bf16[2,2,2,3,128,128]{5,4,3,2,1,0:T(8,128)(2,1)}, u32[]{:S(2)}) copy-start(bf16[2,2,2,3,128,128]{5,4,3,2,1,0:T(8,128)(2,1)} %param.23) | copy-start | bytes 2359300
  69.5 3.9 %collective-permute-start = (bf16[2,384]{1,0:T(2,128)(2,1)S(1)}, bf16[2,384]{1,0:T(2,128)(2,1)S(1)}, u32[]{:S(2)}, u32[]{:S(2)}) collective-permute-start(bf16[2,384]{1,0:T(2,128)(2,1)S(1)} %get-tuple-element.353), channel_id=1, source_target_pairs={{0,4},{4,8},{8,12},{1,5},{5,9},{9,13},{2,6},{6,10},{10,14},{3,7},{... | collective-permute-start | bytes 4616 | tf_op jit(solution)/shard_map/ppermute | solution.py:18
  72.1 5.5 %collective-permute-start.1 = (bf16[2,384]{1,0:T(2,128)(2,1)S(1)}, bf16[2,384]{1,0:T(2,128)(2,1)S(1)}, u32[]{:S(2)}, u32[]{:S(2)}) collective-permute-start(bf16[2,384]{1,0:T(2,128)(2,1)S(1)} %get-tuple-element.354), channel_id=1, source_target_pairs={{4,0},{8,4},{12,8},{5,1},{9,5},{13,9},{6,2},{10,6},{14,10},{7,3},{... | collective-permute-start | bytes 4616 | tf_op jit(solution)/shard_map/ppermute | solution.py:20
  114.7 0.9 copy-start.23
  115.7 0.6 copy-start.22
  116.4 1.7 copy-start.3
  118.9 33.3 %copy-start = (bf16[256,2048]{1,0:T(8,128)(2,1)S(1)}, bf16[256,2048]{1,0:T(8,128)(2,1)}, u32[]{:S(2)}) copy-start(bf16[256,2048]{1,0:T(8,128)(2,1)} %all-gather.31.cloned.1.call-done) | copy-start | bytes 3145732
  118.9 33.3 %copy-start.10 = (f32[1,2048]{1,0:T(1,128)S(1)}, f32[1,2048]{1,0:T(1,128)}, u32[]{:S(2)}) copy-start(f32[1,2048]{1,0:T(1,128)} %copy-done.9) | copy-start | bytes 24580
  118.9 33.3 %copy-start.28 = (f32[256]{0:T(256)S(1)}, f32[256]{0:T(256)}, u32[]{:S(2)}) copy-start(f32[256]{0:T(256)} %copy-done.27) | copy-start | bytes 3076
  156.6 27.1 %copy-start.20 = (f32[384]{0:T(512)S(1)}, f32[384]{0:T(512)}, u32[]{:S(2)}) copy-start(f32[384]{0:T(512)} %get-tuple-element.273) | copy-start | bytes 4612
  156.6 27.2 %copy-start.21 = (f32[384]{0:T(512)S(1)}, f32[384]{0:T(512)}, u32[]{:S(2)}) copy-start(f32[384]{0:T(512)} %get-tuple-element.276) | copy-start | bytes 4612
  156.6 80.3 %copy-start.7 = (f32[1,2048]{1,0:T(1,128)S(1)}, f32[1,2048]{1,0:T(1,128)}, u32[]{:S(2)}) copy-start(f32[1,2048]{1,0:T(1,128)} %get-tuple-element.403) | copy-start | bytes 24580
  156.6 41.7 %all-gather.33.cloned.1.call-start = ((), (), s32[]{:S(2)}) async-start(), calls=%async_computation.4 | async-start | bytes 1310720 | tf_op jit(solution)/shard_map/all_gather | solution.py:75
  181.5 55.5 %all-gather.41.cloned.1.call-start = ((), (), s32[]{:S(2)}) async-start(), calls=%async_computation.9 | async-start | bytes 1966080 | tf_op jit(solution)/shard_map/all_gather | solution.py:79
  182.2 139.5 %all-gather.43.cloned.1.call-start = ((), (), s32[]{:S(2)}) async-start(), calls=%async_computation.10 | async-start | bytes 1966080 | tf_op jit(solution)/shard_map/all_gather | solution.py:84
  183.0 138.7 %all-gather.45.cloned.1.call-start = ((), (), s32[]{:S(2)}) async-start(), calls=%async_computation.11 | async-start | bytes 1966080 | tf_op jit(solution)/shard_map/all_gather | solution.py:141
  183.7 165.8 %reduce-scatter.5.cloned.1.call-start = ((), (), s32[]{:S(2)}) async-start(), calls=%async_computation.5 | async-start | bytes 1310720 | tf_op jit(solution)/shard_map/reduce_scatter | solution.py:144
  199.8 39.6 %copy-start.25 = (f32[256]{0:T(256)}, f32[256]{0:T(256)S(1)}, u32[]{:S(2)}) copy-start(f32[256]{0:T(256)S(1)} %add_rsqrt_fusion) | copy-start | bytes 3076
  236.9 10.7 %copy-start.11 = (f32[384]{0:T(512)S(1)}, f32[384]{0:T(512)}, u32[]{:S(2)}) copy-start(f32[384]{0:T(512)} %get-tuple-element.266) | copy-start | bytes 4612
  236.9 10.7 %copy-start.12 = (f32[384]{0:T(512)S(1)}, f32[384]{0:T(512)}, u32[]{:S(2)}) copy-start(f32[384]{0:T(512)} %get-tuple-element.271) | copy-start | bytes 4612
  236.9 10.7 %copy-start.13 = (f32[384]{0:T(512)S(1)}, f32[384]{0:T(512)}, u32[]{:S(2)}) copy-start(f32[384]{0:T(512)} %get-tuple-element.272) | copy-start | bytes 4612
  239.4 8.6 %copy-start.31 = (bf16[2,2,2,3,128,128]{5,4,3,2,1,0:T(8,128)(2,1)S(1)}, bf16[2,2,2,3,128,128]{5,4,3,2,1,0:T(8,128)(2,1)}, u32[]{:S(2)}) copy-start(bf16[2,2,2,3,128,128]{5,4,3,2,1,0:T(8,128)(2,1)} %param.23) | copy-start | bytes 2359300
  239.5 3.9 %collective-permute-start.2 = (bf16[2,384]{1,0:T(2,128)(2,1)S(1)}, bf16[2,384]{1,0:T(2,128)(2,1)S(1)}, u32[]{:S(2)}, u32[]{:S(2)}) collective-permute-start(bf16[2,384]{1,0:T(2,128)(2,1)S(1)} %get-tuple-element.341), channel_id=1, source_target_pairs={{0,4},{4,8},{8,12},{1,5},{5,9},{9,13},{2,6},{6,10},{10,14},{3,7},{... | collective-permute-start | bytes 4616 | tf_op jit(solution)/shard_map/ppermute | solution.py:18
  242.1 5.5 %collective-permute-start.3 = (bf16[2,384]{1,0:T(2,128)(2,1)S(1)}, bf16[2,384]{1,0:T(2,128)(2,1)S(1)}, u32[]{:S(2)}, u32[]{:S(2)}) collective-permute-start(bf16[2,384]{1,0:T(2,128)(2,1)S(1)} %get-tuple-element.342), channel_id=1, source_target_pairs={{4,0},{8,4},{12,8},{5,1},{9,5},{13,9},{6,2},{10,6},{14,10},{7,3},{... | collective-permute-start | bytes 4616 | tf_op jit(solution)/shard_map/ppermute | solution.py:20
  284.8 1.7 copy-start.4
  287.3 34.3 %copy-start.1 = (bf16[256,2048]{1,0:T(8,128)(2,1)S(1)}, bf16[256,2048]{1,0:T(8,128)(2,1)}, u32[]{:S(2)}) copy-start(bf16[256,2048]{1,0:T(8,128)(2,1)} %all-gather.33.cloned.1.call-done) | copy-start | bytes 3145732
  287.4 34.3 %copy-start.8 = (f32[1,2048]{1,0:T(1,128)S(1)}, f32[1,2048]{1,0:T(1,128)}, u32[]{:S(2)}) copy-start(f32[1,2048]{1,0:T(1,128)} %get-tuple-element.403) | copy-start | bytes 24580
  287.4 34.3 %copy-start.26 = (f32[256]{0:T(256)S(1)}, f32[256]{0:T(256)}, u32[]{:S(2)}) copy-start(f32[256]{0:T(256)} %copy-done.25) | copy-start | bytes 3076
  321.7 27.8 %copy-start.2 = (bf16[256,512]{1,0:T(8,128)(2,1)S(1)}, bf16[256,512]{1,0:T(8,128)(2,1)}, u32[]{:S(2)}) copy-start(bf16[256,512]{1,0:T(8,128)(2,1)} %add_convert_fusion.1) | copy-start | bytes 786436
Sparse Core Ops, SparseCore 0:
  8.9 19.4 all-gather.30
  29.9 37.0 all-gather.34
  68.5 36.0 all-gather.36
  106.0 36.0 all-gather.38
  156.7 22.8 reduce-scatter.2
  181.6 16.6 all-gather.32
  199.9 37.0 all-gather.40
  238.5 36.0 all-gather.42
  276.1 36.0 all-gather.44
  326.4 23.0 reduce-scatter.4
where the time goes:
time: 360 us; the launch traced here: 358 us
  waiting for transfers between devices  158 us (44%)
  blocking collectives  97.5 us (27%)
  local copies, waits for them, and re-layouts  35.6 us (10%)
  other arithmetic  24.8 us (7%)
  between operations  16.9 us (5%)
  matrix products  16.4 us (5%)
  starting transfers between devices  8.37 us (2%)
    all_gather x8, blocking collectives, carried_in(): gathered = jax.tree.map(lambda a: lax.all_gather(a, axis), part)  97.5 us
    all_gather x2, waiting for transfers between devices, local(): lax.all_gather(convolution_in_weight[layer_index], 'sp', axis=0, tiled=True)  74.2 us
    reduce_scatter x2, waiting for transfers between devices, local(): lax.psum_scatter(partials.astype(jnp.float32).astype(jnp.bfloat16), 'tp',...  46 us
    all_gather x2, waiting for transfers between devices, local(): features = lax.all_gather(stream, 'tp', axis=1, tiled=True)  27 us
    rev x4, local copies, waits for them, and re-layouts, local(): lax.associative_scan(combine_pairs, (jnp.exp(decay_logarithm), driven), r...  11.6 us
    slice x220, local copies, waits for them, and re-layouts, local(): lax.associative_scan(combine_pairs, (jnp.exp(decay_logarithm), driven), r...  10.5 us
    dot_general x2, matrix products, local(): jnp.dot(gated, lax.all_gather(output_weight[layer_index], 'sp', axis=1, t...  8.97 us
    ppermute x2, waiting for transfers between devices, extended(): lax.ppermute(head, axis, [((i + 1) % count, i) for i in range(ends)])  8.32 us
  transfers between devices with their start and end apart: 14, of which 8 were waited for; matrix products, arithmetic and copies ran while one was open for 18% of the time, Pallas kernels for 0%

commit v1 on v0

--- a/solution.py
+++ b/solution.py
@@ -72,7 +72,8 @@
     at_first = (positions == 0)[:, None]
     at_last = (positions == seq_length - 1)[:, None]
     for layer_index in range(convolution_in_weight.shape[0]):
-        features = lax.all_gather(stream, "tp", axis=1, tiled=True)
+        parts = lax.all_gather(stream, "tp", axis=0, tiled=False)
+        features = jnp.concatenate(parts, axis=1)
         normed = rms_norm(features, layer_norm_gain[layer_index])
         acc_x = jnp.dot(
             normed,

time: 360 us -> 506 us (1.41)
  local copies, waits for them, and re-layouts: 35.6 us -> 132 us
  other arithmetic: 24.8 us -> 73.2 us
  matrix products: 16.4 us -> 22.9 us
    slice x220, local copies, waits for them, and re-layouts: 10.5 us -> 71.9 us  [local(): lax.associative_scan(combine_pairs, (jnp.exp(decay_logarithm), driven), r...]
    pad x112, local copies, waits for them, and re-layouts: 5.35 us -> 29.2 us  [local(): lax.associative_scan(combine_pairs, (jnp.exp(decay_logarithm), driven), r...]
    add x60, other arithmetic: 5.93 us -> 23.6 us  [local(): lax.associative_scan(combine_pairs, (jnp.exp(decay_logarithm), driven), r...]
    add x58, other arithmetic: 1.14 us -> 14.2 us  [combine_pairs(): return (earlier[0] * latter[0], latter[0] * earlier[1] + latter[1])]
    concatenate x56, other arithmetic: 1.96 us -> 14.1 us  [local(): lax.associative_scan(combine_pairs, (jnp.exp(decay_logarithm), driven), r...]
    all_gather x2, waiting for transfers between devices: 74.2 us -> 66.2 us  [local(): lax.all_gather(convolution_in_weight[layer_index], 'sp', axis=0, tiled=True)]
    convert_element_type x0 -> x4, other arithmetic: none -> 6.38 us  [the longest x2 5.7 us: rms_norm(): floats = values.astype(jnp.float32)]
  transfers between devices with their start and end apart: 14 -> 14, of which waited for: 8 -> 8; matrix products, arithmetic and copies ran while one was open for 18% -> 42% of each run, Pallas kernels for 0% -> 0%
where the time goes in v1:
time: 506 us; the launch traced here: 502 us
  waiting for transfers between devices  153 us (30%)
  local copies, waits for them, and re-layouts  132 us (26%)
  blocking collectives  96.2 us (19%)
  other arithmetic  73.2 us (14%)
  matrix products  22.9 us (5%)
  between operations  17 us (3%)
  starting transfers between devices  7.93 us (2%)
    all_gather x8, blocking collectives, carried_in(): gathered = jax.tree.map(lambda a: lax.all_gather(a, axis), part)  96.2 us
    slice x220, local copies, waits for them, and re-layouts, local(): lax.associative_scan(combine_pairs, (jnp.exp(decay_logarithm), driven), r...  71.9 us
    all_gather x2, waiting for transfers between devices, local(): lax.all_gather(convolution_in_weight[layer_index], 'sp', axis=0, tiled=True)  66.2 us
    reduce_scatter x2, waiting for transfers between devices, local(): lax.psum_scatter(partials.astype(jnp.float32).astype(jnp.bfloat16), 'tp',...  46.5 us
    pad x112, local copies, waits for them, and re-layouts, local(): lax.associative_scan(combine_pairs, (jnp.exp(decay_logarithm), driven), r...  29.2 us
    all_gather x2, waiting for transfers between devices, local(): parts = lax.all_gather(stream, 'tp', axis=0, tiled=False)  28.7 us
    add x60, other arithmetic, local(): lax.associative_scan(combine_pairs, (jnp.exp(decay_logarithm), driven), r...  23.6 us
    add x58, other arithmetic, combine_pairs(): return (earlier[0] * latter[0], latter[0] * earlier[1] + latter[1])  14.2 us
  transfers between devices with their start and end apart: 14, of which 8 were waited for; matrix products, arithmetic and copies ran while one was open for 42% of the time, Pallas kernels for 0%

profile of v1, /device:TPU:0, one launch (start us, length us, event | category | flops | bytes accessed | tf_op | source)
XLA Modules:
  0.0 502.1 jit_solution(7490269021349649992)
XLA Ops:
  7.3 2.1 fusion.199
  14.2 14.1 %all-gather.33.cloned.1.call-done = bf16[1024,512]{1,0:T(8,128)(2,1)} async-done(((bf16[256,512]{1,0:T(8,128)(2,1)}), bf16[1024,512]{1,0:T(8,128)(2,1)}) %all-gather.33.cloned.1.call-update) | async-done | bytes 1048592 | tf_op jit(solution)/shard_map/all_gather | solution.py:75
  28.3 2.8 convert_bitcast_fusion
  31.2 2.0 copy.89
  33.9 33.1 %all-gather.35.cloned.1.call-done = bf16[1,2048,384]{2,1,0:T(8,128)(2,1)} async-done(((bf16[1,512,384]{2,1,0:T(8,128)(2,1)}), bf16[1,2048,384]{2,1,0:T(8,128)(2,1)}) %all-gather.35.cloned.1.call-update) | async-done | bytes 1572880 | tf_op jit(solution)/shard_map/all_gather | solution.py:80
  67.0 2.1 fusion.39
  69.1 2.5 collective-permute-start
  73.0 4.2 collective-permute-done.1
  85.3 2.1 convert_multiply_fusion.4
  123.5 12.3 %all-gather.17 = f32[4,1,384]{2,1,0:T(1,128)S(1)} all-gather(f32[1,1,384]{2,1,0:T(1,128)S(1)} %add_bitcast_fusion.6), channel_id=5, replica_groups=mesh['grp'=2,'sp'=4,'tp'=4] {'sp'}, dimensions={0}, use_global_device_ids=true | all-gather | bytes 7680 | tf_op jit(solution)/shard_map/all_gather | solution.py:31
  138.6 11.9 %all-gather.16 = f32[4,1,384]{2,1,0:T(1,128)S(1)} all-gather(f32[1,1,384]{2,1,0:T(1,128)S(1)} %add_bitcast_fusion.7), channel_id=4, replica_groups=mesh['grp'=2,'sp'=4,'tp'=4] {'sp'}, dimensions={0}, use_global_device_ids=true | all-gather | bytes 7680 | tf_op jit(solution)/shard_map/all_gather | solution.py:31
  159.5 2.0 pad.433
  172.4 2.4 slice.1256
  174.9 2.4 slice.1318
  182.9 1.8 fusion.119
  185.9 1.6 pad_maximum_fusion.3
  187.5 2.5 pad.454
  190.8 1.8 add.997
  193.3 11.9 %all-gather.19 = f32[4,1,384]{2,1,0:T(1,128)S(1)} all-gather(f32[1,1,384]{2,1,0:T(1,128)S(1)} %add_bitcast_fusion.4), channel_id=7, replica_groups=mesh['grp'=2,'sp'=4,'tp'=4] {'sp'}, dimensions={0}, use_global_device_ids=true | all-gather | bytes 7680 | tf_op jit(solution)/shard_map/all_gather | solution.py:31
  206.0 11.9 %all-gather.18 = f32[4,1,384]{2,1,0:T(1,128)S(1)} all-gather(f32[1,1,384]{2,1,0:T(1,128)S(1)} %add_bitcast_fusion.5), channel_id=6, replica_groups=mesh['grp'=2,'sp'=4,'tp'=4] {'sp'}, dimensions={0}, use_global_device_ids=true | all-gather | bytes 7680 | tf_op jit(solution)/shard_map/all_gather | solution.py:31
  218.2 2.6 rev.16
  220.8 2.6 rev.17
  223.4 4.4 convolution_convert_fusion.1
  227.9 23.2 %reduce-scatter.3.cloned.1.call-done = bf16[256,512]{1,0:T(8,128)(2,1)} async-done(((bf16[256,2048]{1,0:T(8,128)(2,1)}), bf16[256,512]{1,0:T(8,128)(2,1)}) %reduce-scatter.3.cloned.1.call-update) | async-done | bytes 262160 | tf_op jit(solution)/shard_map/reduce_scatter | solution.py:145
  251.2 1.8 add_convert_fusion.1
  255.3 14.5 %all-gather.41.cloned.1.call-done = bf16[1024,512]{1,0:T(8,128)(2,1)} async-done(((bf16[256,512]{1,0:T(8,128)(2,1)}), bf16[1024,512]{1,0:T(8,128)(2,1)}) %all-gather.41.cloned.1.call-update) | async-done | bytes 1048592 | tf_op jit(solution)/shard_map/all_gather | solution.py:75
  269.8 2.8 bitcast_convert_fusion
  272.7 2.0 copy.103
  275.4 33.1 %all-gather.43.cloned.1.call-done = bf16[1,2048,384]{2,1,0:T(8,128)(2,1)} async-done(((bf16[1,512,384]{2,1,0:T(8,128)(2,1)}), bf16[1,2048,384]{2,1,0:T(8,128)(2,1)}) %all-gather.43.cloned.1.call-update) | async-done | bytes 1572880 | tf_op jit(solution)/shard_map/all_gather | solution.py:80
  308.5 2.1 fusion.48
  310.6 2.5 collective-permute-start.2
  314.5 4.2 collective-permute-done.3
  326.9 2.1 convert_multiply_fusion.2
  365.4 12.4 %all-gather.21 = f32[4,1,384]{2,1,0:T(1,128)S(1)} all-gather(f32[1,1,384]{2,1,0:T(1,128)S(1)} %add_bitcast_fusion.2), channel_id=13, replica_groups=mesh['grp'=2,'sp'=4,'tp'=4] {'sp'}, dimensions={0}, use_global_device_ids=true | all-gather | bytes 7680 | tf_op jit(solution)/shard_map/all_gather | solution.py:31
  380.5 11.9 %all-gather.20 = f32[4,1,384]{2,1,0:T(1,128)S(1)} all-gather(f32[1,1,384]{2,1,0:T(1,128)S(1)} %add_bitcast_fusion.3), channel_id=12, replica_groups=mesh['grp'=2,'sp'=4,'tp'=4] {'sp'}, dimensions={0}, use_global_device_ids=true | all-gather | bytes 7680 | tf_op jit(solution)/shard_map/all_gather | solution.py:31
  401.7 2.0 pad.497
  414.7 2.4 slice.1436
  417.1 2.4 slice.1498
  425.1 1.8 fusion.117
  427.0 2.5 pad.519
  431.9 2.0 add.1085
  434.5 11.9 %all-gather.23 = f32[4,1,384]{2,1,0:T(1,128)S(1)} all-gather(f32[1,1,384]{2,1,0:T(1,128)S(1)} %add_bitcast_fusion), channel_id=15, replica_groups=mesh['grp'=2,'sp'=4,'tp'=4] {'sp'}, dimensions={0}, use_global_device_ids=true | all-gather | bytes 7680 | tf_op jit(solution)/shard_map/all_gather | solution.py:31
  447.2 11.9 %all-gather.22 = f32[4,1,384]{2,1,0:T(1,128)S(1)} all-gather(f32[1,1,384]{2,1,0:T(1,128)S(1)} %add_bitcast_fusion.1), channel_id=14, replica_groups=mesh['grp'=2,'sp'=4,'tp'=4] {'sp'}, dimensions={0}, use_global_device_ids=true | all-gather | bytes 7680 | tf_op jit(solution)/shard_map/all_gather | solution.py:31
  459.2 2.6 rev.18
  461.8 3.9 rev.19
  465.7 4.6 convolution_convert_fusion
  470.3 23.2 %reduce-scatter.5.cloned.1.call-done = bf16[256,512]{1,0:T(8,128)(2,1)} async-done(((bf16[256,2048]{1,0:T(8,128)(2,1)}), bf16[256,512]{1,0:T(8,128)(2,1)}) %reduce-scatter.5.cloned.1.call-update) | async-done | bytes 262160 | tf_op jit(solution)/shard_map/reduce_scatter | solution.py:145
  493.5 1.7 add_convert_fusion
  (822 shorter events, 162.4 us)
Async XLA Ops:
  6.5 21.8 %all-gather.33.cloned.1.call-start = ((), (), s32[]{:S(2)}) async-start(), calls=%async_computation.4 | async-start | bytes 1310720 | tf_op jit(solution)/shard_map/all_gather | solution.py:75
  7.3 59.7 %all-gather.35.cloned.1.call-start = ((), (), s32[]{:S(2)}) async-start(), calls=%async_computation.5 | async-start | bytes 1966080 | tf_op jit(solution)/shard_map/all_gather | solution.py:80
  9.4 214.0 %all-gather.37.cloned.1.call-start = ((), (), s32[]{:S(2)}) async-start(), calls=%async_computation.6 | async-start | bytes 1966080 | tf_op jit(solution)/shard_map/all_gather | solution.py:85
  10.5 212.9 %all-gather.39.cloned.1.call-start = ((), (), s32[]{:S(2)}) async-start(), calls=%async_computation.7 | async-start | bytes 1966080 | tf_op jit(solution)/shard_map/all_gather | solution.py:142
  11.6 239.5 %reduce-scatter.3.cloned.1.call-start = ((), (), s32[]{:S(2)}) async-start(), calls=%async_computation.2 | async-start | bytes 1310720 | tf_op jit(solution)/shard_map/reduce_scatter | solution.py:145
  13.6 71.7 %copy-start.113 = (pred[256]{0:T(512)(128)(4,1)}, pred[256]{0:T(512)(128)(4,1)S(1)}, u32[]{:S(2)}) copy-start(pred[256]{0:T(512)(128)(4,1)S(1)} %get-tuple-element.485) | copy-start | bytes 772
  13.6 71.7 %copy-start.115 = (pred[256]{0:T(512)(128)(4,1)}, pred[256]{0:T(512)(128)(4,1)S(1)}, u32[]{:S(2)}) copy-start(pred[256]{0:T(512)(128)(4,1)S(1)} %get-tuple-element.486) | copy-start | bytes 772
  69.1 3.8 collective-permute-start
  71.6 5.5 %collective-permute-start.1 = (bf16[2,384]{1,0:T(2,128)(2,1)S(1)}, bf16[2,384]{1,0:T(2,128)(2,1)S(1)}, u32[]{:S(2)}, u32[]{:S(2)}) collective-permute-start(bf16[2,384]{1,0:T(2,128)(2,1)S(1)} %get-tuple-element.354), channel_id=1, source_target_pairs={{4,0},{8,4},{12,8},{5,1},{9,5},{13,9},{6,2},{10,6},{14,10},{7,3},{... | collective-permute-start | bytes 4616 | tf_op jit(solution)/shard_map/ppermute | solution.py:20
  123.3 27.3 %copy-start.58 = (f32[2,384]{1,0:T(2,128)S(1)}, f32[2,384]{1,0:T(2,128)}, u32[]{:S(2)}) copy-start(f32[2,384]{1,0:T(2,128)} %pad_add_fusion.5) | copy-start | bytes 9220
  123.3 27.3 %copy-start.84 = (f32[1,384]{1,0:T(1,128)S(1)}, f32[1,384]{1,0:T(1,128)}, u32[]{:S(2)}) copy-start(f32[1,384]{1,0:T(1,128)} %get-tuple-element.447) | copy-start | bytes 4612
  123.3 27.3 %copy-start.85 = (f32[1,384]{1,0:T(1,128)S(1)}, f32[1,384]{1,0:T(1,128)}, u32[]{:S(2)}) copy-start(f32[1,384]{1,0:T(1,128)} %get-tuple-element.448) | copy-start | bytes 4612
  123.3 27.3 %copy-start.43 = (f32[3,384]{1,0:T(4,128)S(1)}, f32[3,384]{1,0:T(4,128)}, u32[]{:S(2)}) copy-start(f32[3,384]{1,0:T(4,128)} %slice.1290) | copy-start | bytes 13828
  123.3 27.3 %copy-start.44 = (f32[3,384]{1,0:T(4,128)S(1)}, f32[3,384]{1,0:T(4,128)}, u32[]{:S(2)}) copy-start(f32[3,384]{1,0:T(4,128)} %slice.1307) | copy-start | bytes 13828
  123.4 27.4 %copy-start.81 = (f32[1,384]{1,0:T(1,128)S(1)}, f32[1,384]{1,0:T(1,128)}, u32[]{:S(2)}) copy-start(f32[1,384]{1,0:T(1,128)} %slice.1607) | copy-start | bytes 4612
  123.4 27.4 %copy-start.79 = (f32[1,384]{1,0:T(1,128)S(1)}, f32[1,384]{1,0:T(1,128)}, u32[]{:S(2)}) copy-start(f32[1,384]{1,0:T(1,128)} %slice.1581) | copy-start | bytes 4612
  123.4 28.1 %copy-start.36 = (f32[7,384]{1,0:T(8,128)S(1)}, f32[7,384]{1,0:T(8,128)}, u32[]{:S(2)}) copy-start(f32[7,384]{1,0:T(8,128)} %slice.1284) | copy-start | bytes 32260
  123.4 28.1 %copy-start.37 = (f32[7,384]{1,0:T(8,128)S(1)}, f32[7,384]{1,0:T(8,128)}, u32[]{:S(2)}) copy-start(f32[7,384]{1,0:T(8,128)} %slice.1309) | copy-start | bytes 32260
  138.5 33.1 %copy-start.5 = (f32[256,384]{1,0:T(8,128)}, f32[256,384]{1,0:T(8,128)S(1)}, u32[]{:S(2)}) copy-start(f32[256,384]{1,0:T(8,128)S(1)} %pad.422) | copy-start | bytes 1179652
  190.8 32.6 %copy-start.6 = (f32[256,384]{1,0:T(8,128)S(1)}, f32[256,384]{1,0:T(8,128)}, u32[]{:S(2)}) copy-start(f32[256,384]{1,0:T(8,128)} %copy-done.5) | copy-start | bytes 1179652
  227.9 27.4 %copy-start.63 = (f32[384]{0:T(512)S(1)}, f32[384]{0:T(512)}, u32[]{:S(2)}) copy-start(f32[384]{0:T(512)} %get-tuple-element.273) | copy-start | bytes 4612
  227.9 27.4 %copy-start.64 = (f32[384]{0:T(512)S(1)}, f32[384]{0:T(512)}, u32[]{:S(2)}) copy-start(f32[384]{0:T(512)} %get-tuple-element.276) | copy-start | bytes 4612
  227.9 42.0 %all-gather.41.cloned.1.call-start = ((), (), s32[]{:S(2)}) async-start(), calls=%async_computation.8 | async-start | bytes 1310720 | tf_op jit(solution)/shard_map/all_gather | solution.py:75
  253.0 55.5 %all-gather.43.cloned.1.call-start = ((), (), s32[]{:S(2)}) async-start(), calls=%async_computation.9 | async-start | bytes 1966080 | tf_op jit(solution)/shard_map/all_gather | solution.py:80
  253.8 211.9 %all-gather.45.cloned.1.call-start = ((), (), s32[]{:S(2)}) async-start(), calls=%async_computation.10 | async-start | bytes 1966080 | tf_op jit(solution)/shard_map/all_gather | solution.py:85
  254.5 211.2 %all-gather.47.cloned.1.call-start = ((), (), s32[]{:S(2)}) async-start(), calls=%async_computation.11 | async-start | bytes 1966080 | tf_op jit(solution)/shard_map/all_gather | solution.py:142
  255.2 238.3 %reduce-scatter.5.cloned.1.call-start = ((), (), s32[]{:S(2)}) async-start(), calls=%async_computation.3 | async-start | bytes 1310720 | tf_op jit(solution)/shard_map/reduce_scatter | solution.py:145
  275.4 43.3 %copy-start.49 = (f32[384]{0:T(512)S(1)}, f32[384]{0:T(512)}, u32[]{:S(2)}) copy-start(f32[384]{0:T(512)} %get-tuple-element.265) | copy-start | bytes 4612
  275.4 43.3 %copy-start.50 = (f32[384]{0:T(512)S(1)}, f32[384]{0:T(512)}, u32[]{:S(2)}) copy-start(f32[384]{0:T(512)} %get-tuple-element.266) | copy-start | bytes 4612
  275.4 43.3 %copy-start.51 = (f32[384]{0:T(512)S(1)}, f32[384]{0:T(512)}, u32[]{:S(2)}) copy-start(f32[384]{0:T(512)} %get-tuple-element.271) | copy-start | bytes 4612
  275.4 43.3 %copy-start.52 = (f32[384]{0:T(512)S(1)}, f32[384]{0:T(512)}, u32[]{:S(2)}) copy-start(f32[384]{0:T(512)} %get-tuple-element.272) | copy-start | bytes 4612
  310.6 3.8 collective-permute-start.2
  313.1 5.5 %collective-permute-start.3 = (bf16[2,384]{1,0:T(2,128)(2,1)S(1)}, bf16[2,384]{1,0:T(2,128)(2,1)S(1)}, u32[]{:S(2)}, u32[]{:S(2)}) collective-permute-start(bf16[2,384]{1,0:T(2,128)(2,1)S(1)} %get-tuple-element.342), channel_id=1, source_target_pairs={{4,0},{8,4},{12,8},{5,1},{9,5},{13,9},{6,2},{10,6},{14,10},{7,3},{... | collective-permute-start | bytes 4616 | tf_op jit(solution)/shard_map/ppermute | solution.py:20
  365.2 27.4 %copy-start.86 = (f32[1,384]{1,0:T(1,128)S(1)}, f32[1,384]{1,0:T(1,128)}, u32[]{:S(2)}) copy-start(f32[1,384]{1,0:T(1,128)} %get-tuple-element.433) | copy-start | bytes 4612
  365.2 27.5 %copy-start.87 = (f32[1,384]{1,0:T(1,128)S(1)}, f32[1,384]{1,0:T(1,128)}, u32[]{:S(2)}) copy-start(f32[1,384]{1,0:T(1,128)} %get-tuple-element.434) | copy-start | bytes 4612
  365.2 27.5 %copy-start.55 = (f32[2,384]{1,0:T(2,128)S(1)}, f32[2,384]{1,0:T(2,128)}, u32[]{:S(2)}) copy-start(f32[2,384]{1,0:T(2,128)} %pad_add_fusion) | copy-start | bytes 9220
  365.2 27.5 %copy-start.57 = (f32[2,384]{1,0:T(2,128)S(1)}, f32[2,384]{1,0:T(2,128)}, u32[]{:S(2)}) copy-start(f32[2,384]{1,0:T(2,128)} %pad_add_fusion.1) | copy-start | bytes 9220
  365.2 27.5 %copy-start.82 = (f32[1,384]{1,0:T(1,128)S(1)}, f32[1,384]{1,0:T(1,128)}, u32[]{:S(2)}) copy-start(f32[1,384]{1,0:T(1,128)} %get-tuple-element.431) | copy-start | bytes 4612
  365.2 27.5 %copy-start.83 = (f32[1,384]{1,0:T(1,128)S(1)}, f32[1,384]{1,0:T(1,128)}, u32[]{:S(2)}) copy-start(f32[1,384]{1,0:T(1,128)} %get-tuple-element.432) | copy-start | bytes 4612
  365.2 27.6 %copy-start.41 = (f32[3,384]{1,0:T(4,128)S(1)}, f32[3,384]{1,0:T(4,128)}, u32[]{:S(2)}) copy-start(f32[3,384]{1,0:T(4,128)} %slice.1470) | copy-start | bytes 13828
  365.2 27.6 %copy-start.42 = (f32[3,384]{1,0:T(4,128)S(1)}, f32[3,384]{1,0:T(4,128)}, u32[]{:S(2)}) copy-start(f32[3,384]{1,0:T(4,128)} %slice.1487) | copy-start | bytes 13828
  365.2 27.6 %copy-start.80 = (f32[1,384]{1,0:T(1,128)S(1)}, f32[1,384]{1,0:T(1,128)}, u32[]{:S(2)}) copy-start(f32[1,384]{1,0:T(1,128)} %slice.1717) | copy-start | bytes 4612
  365.2 27.7 %copy-start.78 = (f32[1,384]{1,0:T(1,128)S(1)}, f32[1,384]{1,0:T(1,128)}, u32[]{:S(2)}) copy-start(f32[1,384]{1,0:T(1,128)} %slice.1691) | copy-start | bytes 4612
  365.2 28.3 %copy-start.34 = (f32[7,384]{1,0:T(8,128)S(1)}, f32[7,384]{1,0:T(8,128)}, u32[]{:S(2)}) copy-start(f32[7,384]{1,0:T(8,128)} %slice.1464) | copy-start | bytes 32260
  365.3 28.3 %copy-start.35 = (f32[7,384]{1,0:T(8,128)S(1)}, f32[7,384]{1,0:T(8,128)}, u32[]{:S(2)}) copy-start(f32[7,384]{1,0:T(8,128)} %slice.1489) | copy-start | bytes 32260
  380.5 33.4 %copy-start.3 = (f32[256,384]{1,0:T(8,128)}, f32[256,384]{1,0:T(8,128)S(1)}, u32[]{:S(2)}) copy-start(f32[256,384]{1,0:T(8,128)S(1)} %pad.486) | copy-start | bytes 1179652
  431.9 33.8 %copy-start.4 = (f32[256,384]{1,0:T(8,128)S(1)}, f32[256,384]{1,0:T(8,128)}, u32[]{:S(2)}) copy-start(f32[256,384]{1,0:T(8,128)} %copy-done.3) | copy-start | bytes 1179652
  465.7 27.8 %copy-start.2 = (bf16[256,512]{1,0:T(8,128)(2,1)S(1)}, bf16[256,512]{1,0:T(8,128)(2,1)}, u32[]{:S(2)}) copy-start(bf16[256,512]{1,0:T(8,128)(2,1)} %add_convert_fusion.1) | copy-start | bytes 786436
  (83 other events, 749.9 us)
Sparse Core Ops, SparseCore 0:
  8.9 19.4 all-gather.32
  29.9 37.0 all-gather.34
  68.5 35.8 all-gather.36
  105.9 35.9 all-gather.38
  228.0 23.1 reduce-scatter.2
  253.1 16.6 all-gather.40
  271.4 37.0 all-gather.42
  310.0 35.8 all-gather.44
  347.5 35.9 all-gather.46
  470.4 23.0 reduce-scatter.4
